TPU v7x, 128 devices: a whole 4x4x4 slice. The times are simulated.
128 devices in a mesh: sp: 16 (over z, y), tp: 8 (over x, core).
Axes of the slice: x: 4, y: 4, z: 4, core: 2. Of those that a mesh axis runs over, the one named last changes fastest.
Arguments:
- stream: bfloat16 [32768, 4096], P('sp', 'tp'), may hold values from -18 to 18
- doc_ids: int32 [32768], P('sp'), may hold values from 0 to 3, never falling along the last dimension, each value on 1 to 12288 neighbouring positions
- norm_gain: bfloat16 [3, 4096], replicated, may hold values from 0.099609375 to 1.8984375
- proj_in: bfloat16 [3, 4096, 1024], P(None, 'tp', 'sp'), may hold values from -0.09375 to 0.09375
- mix_pool: bfloat16 [3, 8, 128, 128], replicated, may hold values from -0.5 to 0.5
- pool_gain: bfloat16 [3, 1024], replicated, may hold values from 0.099609375 to 1.8984375
- proj_out: bfloat16 [3, 1024, 4096], P(None, 'sp', 'tp'), may hold values from -0.1875 to 0.1875
Outputs:
- stream_out: bfloat16 [32768, 4096], P('sp', 'tp')
Inputs may be any that keep to these rules, and one draw needn't show every extreme that they name: `doc_ids`: document numbers never fall along the sequence; each document holds 1 to 12288 positions, one exactly that many.
All inputs are finite; a program needn't handle non-finite values.
Results may differ from a plain program's by a relative error of at most 0.02.
Values may be sent and summed in bfloat16 or wider, within the bound.
A program may use at most 64 MiB of HBM per device.

v0:
```python
import jax
import jax.numpy as jnp
from jax import lax
from jax.experimental import pallas as pl
from jax.experimental.pallas import tpu as pltpu
from jax.sharding import PartitionSpec as P

MESH = pl.DeviceIdType.MESH
F32 = jnp.float32
BF16 = jnp.bfloat16

D = 4096
POOL = 1024
GROUP = 128
GROUPS = POOL // GROUP
LAYERS = 3
MATS = 2 * LAYERS
TOK = 2048
COLS = 512
PART = TOK // 4
WIDE = 4 * COLS
HALO = 48
LEAD = 16
CHUNKS = 5
CH = (HALO + PART) // CHUNKS
WINDOWS = (2, 4, 8, 16)
EPS = 1e-06


def kernel(
    stream, docs, norm_gain, w_in, mix_pool, pool_gain, out,
    wbuf, hbuf, own, got, ssown, ssgot, gbuf, zbuf, mbuf, sqbuf, band, inv, ext,
    loc_w, loc_h, loc_hh, loc_o,
    s0, r0, s1, r1, s1f, r1f, s2, r2, s2f, r2f, s3, r3,
    sh, rh, shh, rhh, sl, rl, sx, rx, sq, rq, so, ro,
):
    sp = lax.axis_index("sp")
    tp = lax.axis_index("tp")
    z, y = sp // 4, sp % 4
    x, core = tp // 2, tp % 2
    half, xl = x // 2, x % 2
    me = xl * 2 + core
    mine = (me + 2 * half) % 4

    def remote(src, dst, send, recv, device):
        return pltpu.make_async_remote_copy(
            src_ref=src, dst_ref=dst, send_sem=send, recv_sem=recv,
            device_id=device, device_id_type=MESH,
        )

    across = (sp, (2 * half + 1 - xl) * 2 + core)
    partner = (sp, (3 - x) * 2 + core)
    sibling = (sp, x * 2 + 1 - core)

    def along_y(d):
        return (z * 4 + (y + d + 4) % 4, tp)

    def along_z(d):
        return (((z + d + 4) % 4) * 4 + y, tp)

    first_axis = (along_y, along_z)
    second_axis = (along_z, along_y)
    steps = (1, -1)

    def shard(m, k, d):
        if k == 0:
            return wbuf.at[m, core, 0, z, (y + d + 4) % 4]
        return wbuf.at[m, core, 1, (z + d + 4) % 4, y]

    def plane(m, k, d, c=None):
        c = core if c is None else c
        if k == 0:
            return wbuf.at[m, c, 0, (z + d + 4) % 4]
        return wbuf.at[m, c, 1, :, (y + d + 4) % 4]

    def plane_half(m, k, d, which):
        part = pl.ds(2 * which, 2)
        if k == 0:
            return wbuf.at[m, core, 0, (z + d + 4) % 4, part]
        return wbuf.at[m, core, 1, part, (y + d + 4) % 4]

    pairs = [(k, j) for k in range(2) for j in range(2)]

    def c_local(m):
        return pltpu.make_async_copy(w_in.at[m], wbuf.at[m, core, xl, z, y], loc_w.at[m])

    def c0(m):
        return remote(w_in.at[m], wbuf.at[m, core, xl, z, y], s0.at[m], r0.at[m], across)

    def c1(m, k, j):
        return remote(shard(m, k, 0), shard(m, k, 0), s1.at[m, k, j], r1.at[m, k, j], first_axis[k](steps[j]))

    def c1f(m, k, j):
        ref = shard(m, k, -steps[j]).at[pl.ds(32 * j, 32)]
        return remote(ref, ref, s1f.at[m, k, j], r1f.at[m, k, j], first_axis[k](steps[j]))

    def c2(m, k, j):
        return remote(plane(m, k, 0), plane(m, k, 0), s2.at[m, k, j], r2.at[m, k, j], second_axis[k](steps[j]))

    def c2f(m, k, j):
        ref = plane_half(m, k, -steps[j], j)
        return remote(ref, ref, s2f.at[m, k, j], r2f.at[m, k, j], second_axis[k](steps[j]))

    def c3(m, k, p):
        ref = plane(m, k, (0, -1, 1, 2)[p])
        return remote(ref, ref, s3.at[m, k, p], r3.at[m, k, p], sibling)

    def row_start(m):
        c_local(m).wait()
        c0(m).wait_recv()
        for k, j in pairs:
            c1(m, k, j).start()

    def row_pass(m):
        for k, j in pairs:
            c1(m, k, j).wait_recv()
            c1f(m, k, j).start()

    def row_end(m):
        for k, j in pairs:
            c1f(m, k, j).wait_recv()

    def row_gather(m):
        row_start(m)
        row_pass(m)
        row_end(m)

    def plane_start(m):
        for k, j in pairs:
            c2(m, k, j).start()
        for k in range(2):
            c3(m, k, 0).start()

    def plane_pass(m):
        for k, j in pairs:
            c2(m, k, j).wait_recv()
            c2f(m, k, j).start()
            c3(m, k, 1 + j).start()

    def plane_end(m):
        for k, j in pairs:
            c2f(m, k, j).wait_recv()
        for k in range(2):
            c3(m, k, 3).start()

    def weights_ready(m):
        for k in range(2):
            for p in range(4):
                c3(m, k, p).wait_recv()

    def peer(j):
        return (me + j) % 4

    def rows_of(c):
        return (HALO, CH - HALO) if c == 0 else (CH * c, CH)

    def h_main(c, j):
        to = peer(j)
        start, size = rows_of(c)
        base = ((to + 2 * half) % 4) * PART + start - HALO
        return remote(
            stream.at[pl.ds(pl.multiple_of(base, 16), size)], hbuf.at[me, pl.ds(start, size)],
            sh.at[c, j], rh.at[c, me], (sp, 4 * half + to),
        )

    def h_main_wait(c, j):
        start, size = rows_of(c)
        ref = hbuf.at[peer(j), pl.ds(start, size)]
        return remote(ref, ref, sh.at[c, j], rh.at[c, peer(j)], (sp, 4 * half + peer(j)))

    def h_main_local(c):
        start, size = rows_of(c)
        base = mine * PART + start - HALO
        return pltpu.make_async_copy(
            stream.at[pl.ds(pl.multiple_of(base, 16), size)], hbuf.at[me, pl.ds(start, size)], loc_h.at[c]
        )

    def h_halo(j):
        to = peer(j)
        quarter = (to + 2 * half) % 4
        base = (quarter * PART + TOK - HALO) % TOK
        to_sp = (sp + 1 - (quarter + 3) // 4) % 16
        return remote(
            stream.at[pl.ds(pl.multiple_of(base, 16), HALO)], hbuf.at[me, pl.ds(0, HALO)],
            shh.at[j], rhh.at[me], (to_sp, 4 * half + to),
        )

    def h_halo_wait(j):
        ref = hbuf.at[peer(j), pl.ds(0, HALO)]
        return remote(ref, ref, shh.at[j], rhh.at[peer(j)], (sp, 4 * half + peer(3)))

    def h_halo_local():
        base = (mine * PART + TOK - HALO) % TOK
        return pltpu.make_async_copy(
            stream.at[pl.ds(pl.multiple_of(base, 16), HALO)], hbuf.at[me, pl.ds(0, HALO)], loc_hh.at[0]
        )

    def labels():
        return remote(docs.at[pl.ds(15, 1)], ext.at[pl.ds(7, 1)], sl.at[0], rl.at[0], ((sp + 1) % 16, tp))

    for m in range(MATS):
        c_local(m).start()
    c0(0).start()
    labels().start()
    for j in range(1, 4):
        h_halo(j).start()

    @pl.when(mine == 0)
    def _():
        h_halo(0).start()

    @pl.when(mine != 0)
    def _():
        h_halo_local().start()

    for c in range(CHUNKS):
        h_main_local(c).start()
        for j in range(1, 4):
            h_main(c, j).start()
        if c == 0:
            c0(1).start()
    for m in range(2, MATS):
        c0(m).start()

    row_start(0)

    zbuf[...] = jnp.zeros_like(zbuf)
    sqbuf[...] = jnp.zeros_like(sqbuf)
    ext[8:24, :] = docs[...]
    labels().wait_recv()
    label_rows = []
    for k in range(5):
        row = (ext[pl.ds(4 * mine + 7 + k, 1), :] + 1).astype(F32)
        if k == 0:
            row = jnp.where(jnp.logical_and(sp == 0, mine == 0), jnp.zeros_like(row), row)
        label_rows.append(row)
    t_id = lax.broadcasted_iota(jnp.int32, (128, 128), 0)
    s_id = lax.broadcasted_iota(jnp.int32, (128, 128), 1)
    back = t_id - s_id
    lane = lax.broadcasted_iota(jnp.int32, (1, 128), 1)
    for c in range(CHUNKS):
        first, off = divmod(128 - HALO - LEAD + CH * c, 128)
        if off == 0:
            window = label_rows[first]
        else:
            window = jnp.where(
                lane < 128 - off,
                pltpu.roll(label_rows[first], 128 - off, 1),
                pltpu.roll(label_rows[first + 1], 128 - off, 1),
            )
        across_lanes = jnp.broadcast_to(window, (128, 128))
        same = jnp.logical_and(across_lanes == across_lanes.T, back >= 0)
        for i, w in enumerate(WINDOWS):
            member = jnp.where(jnp.logical_and(same, back < w), 1.0, 0.0).astype(F32)
            count = jnp.sum(member, axis=1, keepdims=True)
            band[c, i] = member[LEAD:].astype(BF16)
            inv[c, i] = jnp.broadcast_to(1.0 / count, (128, 128))[LEAD:]

    row_pass(0)
    row_end(0)
    plane_start(0)
    row_gather(1)
    plane_pass(0)
    plane_start(1)
    plane_end(0)
    weights_ready(0)

    def rows_at(c):
        return pl.ds(pl.multiple_of(c * CH, 16), CH)

    def squares_of(wide):
        total = None
        for k in range(COLS // 128):
            piece = wide[:, k * 128 : (k + 1) * 128]
            total = piece * piece if total is None else total + piece * piece
        return total

    def gain_of(l, b):
        at = pl.ds(pl.multiple_of(half * WIDE + b * COLS, COLS), COLS)
        return norm_gain[l : l + 1, at].astype(F32)

    def send_x(s):
        return remote(own.at[s], got.at[s], sx.at[s], rx.at[s], partner)

    def send_sq(s):
        return remote(ssown.at[s], ssgot.at[s], sq.at[s], rq.at[s], partner)

    def project(l, s, squares):
        sqbuf[0:CH, :] = squares
        ssown[s] = jnp.broadcast_to(jnp.sum(sqbuf[...].T, axis=0, keepdims=True), (8, 128))
        send_sq(s).start()
        for n in range(4):
            rhs = jnp.concatenate(
                [wbuf[2 * l, b % 2, b // 2, n].reshape(256, COLS) for b in range(4)], axis=1
            )
            part = lax.dot_general(
                gbuf[...], rhs, (((1,), (1,)), ((), ())), preferred_element_type=F32
            )
            own[s, :, n * 256 : (n + 1) * 256] = part.astype(BF16)
        send_x(s).start()

    def mix(l, c, s):
        send_sq(s).wait_recv()
        send_x(s).wait_recv()
        scale = lax.rsqrt((ssown[s] + ssgot[s]) / D + EPS)[0:1]
        scale = jnp.broadcast_to(scale, (128, 128)).T[0:CH]
        zbuf[0:LEAD, :] = zbuf[CH : CH + LEAD, :]
        for i in range(GROUPS):
            at = slice(i * GROUP, (i + 1) * GROUP)
            summed = own[s, :, at].astype(F32) + got[s, :, at].astype(F32)
            zbuf[LEAD:, at] = (summed * scale).astype(BF16)
        for i in range(GROUPS):
            at = slice(i * GROUP, (i + 1) * GROUP)
            values = zbuf[:, at]
            total = jnp.dot(band[c, i % 4], values, preferred_element_type=F32)
            pooled = (total * inv[c, i % 4] - zbuf[LEAD:, at].astype(F32)).astype(BF16)
            blended = jnp.dot(pooled, mix_pool[l, i], preferred_element_type=F32)
            mbuf[:, at] = (blended * pool_gain[l : l + 1, at].astype(F32)).astype(BF16)

    def update(l, c, last):
        rows = rows_at(c)
        squares = None
        for b in range(4):
            weights = wbuf[2 * l + 1, b % 2, b // 2].reshape(POOL, COLS)
            change = jnp.dot(mbuf[...], weights, preferred_element_type=F32)
            new = (hbuf[b, rows, :].astype(F32) + change).astype(BF16)
            hbuf[b, rows, :] = new
            if not last:
                wide = new.astype(F32)
                squares = squares_of(wide) if squares is None else squares + squares_of(wide)
                gbuf[:, b * COLS : (b + 1) * COLS] = (wide * gain_of(l + 1, b)).astype(BF16)
        return squares

    def wait_rows(c):
        h_main_local(c).wait()
        for j in range(1, 4):
            h_main_wait(c, j).wait_recv()

    @pl.when(mine == 0)
    def _():
        h_halo_wait(0).wait_recv()

    @pl.when(mine != 0)
    def _():
        h_halo_local().wait()

    for j in range(1, 4):
        h_halo_wait(j).wait_recv()

    def enter(c, carry):
        for k in range(CHUNKS):

            @pl.when(c == k)
            def _(k=k):
                wait_rows(k)

        rows = rows_at(c)
        squares = None
        for b in range(4):
            wide = hbuf[b, rows, :].astype(F32)
            squares = squares_of(wide) if squares is None else squares + squares_of(wide)
            gbuf[:, b * COLS : (b + 1) * COLS] = (wide * gain_of(0, b)).astype(BF16)
        project(0, c, squares)
        return carry

    lax.fori_loop(0, CHUNKS, enter, 0)

    def advance(m, prepare):
        if m + 1 < MATS and prepare:
            row_gather(m + 1)
        plane_pass(m)
        if m + 1 < MATS:
            plane_start(m + 1)
        plane_end(m)
        weights_ready(m)

    def out_rows(c):
        start, size = rows_of(c)
        return start, size, mine * PART + start - HALO

    def send_out(c, j):
        start, size, base = out_rows(c)
        to = peer(j)
        return remote(
            hbuf.at[to, pl.ds(start, size)], out.at[pl.ds(pl.multiple_of(base, 16), size)],
            so.at[c, j], ro.at[c, me], (sp, 4 * half + to),
        )

    def keep_out(c):
        start, size, base = out_rows(c)
        return pltpu.make_async_copy(
            hbuf.at[me, pl.ds(start, size)], out.at[pl.ds(pl.multiple_of(base, 16), size)], loc_o.at[c]
        )

    def wait_out(c, j):
        start, size, _ = out_rows(c)
        frm = peer(j)
        base = ((frm + 2 * half) % 4) * PART + start - HALO
        ref = out.at[pl.ds(pl.multiple_of(base, 16), size)]
        return remote(ref, ref, so.at[c, j], ro.at[c, frm], (sp, 4 * half + frm))

    for l in range(LAYERS):
        last = l == LAYERS - 1
        advance(2 * l + 1, True)
        if not last:
            advance(2 * l + 2, True)

        def one(c, carry, l=l, last=last):
            s = l * CHUNKS + c
            mix(l, c, s)
            squares = update(l, c, last)
            if not last:
                project(l + 1, s + CHUNKS, squares)
            else:
                for k in range(CHUNKS):

                    @pl.when(c == k)
                    def _(k=k):
                        for j in range(1, 4):
                            send_out(k, j).start()
                        keep_out(k).start()

            return carry

        lax.fori_loop(0, CHUNKS, one, 0)

    for m in range(MATS):
        c0(m).wait_send()
        for k, j in pairs:
            c1(m, k, j).wait_send()
            c1f(m, k, j).wait_send()
            c2(m, k, j).wait_send()
            c2f(m, k, j).wait_send()
        for k in range(2):
            for p in range(4):
                c3(m, k, p).wait_send()
    labels().wait_send()
    for j in range(1, 4):
        h_halo(j).wait_send()

    @pl.when(mine == 0)
    def _():
        h_halo(0).wait_send()

    for c in range(CHUNKS):
        for j in range(1, 4):
            h_main(c, j).wait_send()
    for s in range(LAYERS * CHUNKS):
        send_x(s).wait_send()
        send_sq(s).wait_send()
    for c in range(CHUNKS):
        keep_out(c).wait()
        for j in range(1, 4):
            send_out(c, j).wait_send()
            wait_out(c, j).wait_recv()


def body(stream, doc_ids, norm_gain, proj_in, mix_pool, pool_gain, proj_out):
    weights = jnp.stack([jnp.swapaxes(proj_in, 1, 2), proj_out], axis=1)
    weights = weights.reshape(MATS, 64, COLS)
    dma = pltpu.SemaphoreType.DMA
    steps = LAYERS * CHUNKS
    vmem = pl.BlockSpec(memory_space=pltpu.VMEM)
    hbm = pl.BlockSpec(memory_space=pl.ANY)
    return pl.pallas_call(
        kernel,
        out_shape=jax.ShapeDtypeStruct((TOK, COLS), BF16),
        in_specs=[hbm, vmem, vmem, hbm, vmem, vmem],
        out_specs=hbm,
        scratch_shapes=[
            pltpu.VMEM((MATS, 2, 2, 4, 4, 64, COLS), BF16),
            pltpu.VMEM((4, HALO + PART, COLS), BF16),
            pltpu.VMEM((steps, CH, POOL), BF16),
            pltpu.VMEM((steps, CH, POOL), BF16),
            pltpu.VMEM((steps, 8, 128), F32),
            pltpu.VMEM((steps, 8, 128), F32),
            pltpu.VMEM((CH, WIDE), BF16),
            pltpu.VMEM((LEAD + CH, POOL), BF16),
            pltpu.VMEM((CH, POOL), BF16),
            pltpu.VMEM((128, 128), F32),
            pltpu.VMEM((CHUNKS, 4, CH, 128), BF16),
            pltpu.VMEM((CHUNKS, 4, CH, 128), F32),
            pltpu.VMEM((24, 128), jnp.int32),
            dma((MATS,)), dma((CHUNKS,)), dma((1,)), dma((CHUNKS,)),
            dma((MATS,)), dma((MATS,)),
            dma((MATS, 2, 2)), dma((MATS, 2, 2)), dma((MATS, 2, 2)), dma((MATS, 2, 2)),
            dma((MATS, 2, 2)), dma((MATS, 2, 2)), dma((MATS, 2, 2)), dma((MATS, 2, 2)),
            dma((MATS, 2, 4)), dma((MATS, 2, 4)),
            dma((CHUNKS, 4)), dma((CHUNKS, 4)), dma((4,)), dma((4,)), dma((1,)), dma((1,)),
            dma((steps,)), dma((steps,)), dma((steps,)), dma((steps,)),
            dma((CHUNKS, 4)), dma((CHUNKS, 4)),
        ],
        compiler_params=pltpu.CompilerParams(
            has_side_effects=True, vmem_limit_bytes=56 * 1024 * 1024
        ),
        name="mixers",
    )(stream, doc_ids.reshape(16, 128), norm_gain, weights, mix_pool, pool_gain)


def solution(mesh):
    in_specs = (P("sp", "tp"), P("sp"), P(), P(None, "tp", "sp"), P(), P(), P(None, "sp", "tp"))
    out_specs = P("sp", "tp")
    return jax.shard_map(body, mesh=mesh, in_specs=in_specs, out_specs=out_specs, check_vma=False)
```

profile of v0, /device:TPU:1, one launch (start us, length us, event | category | flops | bytes accessed | tf_op | source)
XLA Modules:
  0.0 177.7 jit_solution(10549694464941744123)
XLA Ops:
  0.0 1.1 pad_maximum_fusion
  1.1 0.8 copy.8
  1.8 172.8 %mixers.1 = bf16[2048,512]{1,0:T(8,128)(2,1)} custom-call(bf16[2048,512]{1,0:T(8,128)(2,1)} %stream.1, s32[16,128]{1,0:T(8,128)} %bitcast.9, bf16[3,4096]{1,0:T(4,128)(2,1)} %norm_gain.1, bf16[6,64,512]{2,1,0:T(8,128)(2,1)} %bitcast.6, bf16[3,8,128,128]{3,2,1,0:T(8,128)(2,1)} %mix_pool.1, bf16[3,1024]{1,0:T(4,128)(2,1)} %pool_gain.1), custom_call_target="tpu_custom_call" | custom-call | tf_op jit(solution)/shard_map/mixers/pallas_call | solution.py:465
  174.7 3.0 %copy.10 = bf16[2048,512]{1,0:T(8,128)(2,1)} copy(bf16[2048,512]{1,0:T(8,128)(2,1)} %mixers.1) | data formatting | bytes 4194304
where the time goes:
time: 178 us
  Pallas kernels  173 us (97%)
  local copies, waits for them, and re-layouts  3.82 us (2%)
    pallas_call x1, Pallas kernels, body(): pl.pallas_call(kernel, out_shape=jax.ShapeDtypeStruct((TOK, COLS), BF16),...  173 us

commit v1 on v0

--- a/solution.py
+++ b/solution.py
@@ -28,7 +28,7 @@
 
 
 def kernel(
-    stream, docs, norm_gain, w_in, mix_pool, pool_gain, out,
+    stream, docs, norm_gain, w_in, w_out, mix_pool, pool_gain, out,
     wbuf, hbuf, own, got, ssown, ssgot, gbuf, zbuf, mbuf, sqbuf, band, inv, ext,
     loc_w, loc_h, loc_hh, loc_o,
     s0, r0, s1, r1, s1f, r1f, s2, r2, s2f, r2f, s3, r3,
@@ -82,10 +82,11 @@
     pairs = [(k, j) for k in range(2) for j in range(2)]
 
     def c_local(m):
-        return pltpu.make_async_copy(w_in.at[m], wbuf.at[m, core, xl, z, y], loc_w.at[m])
+        source = w_in if m % 2 == 0 else w_out
+        return pltpu.make_async_copy(source.at[m // 2], wbuf.at[m, core, xl, z, y], loc_w.at[m])
 
     def c0(m):
-        return remote(w_in.at[m], wbuf.at[m, core, xl, z, y], s0.at[m], r0.at[m], across)
+        return remote(wbuf.at[m, core, xl, z, y], wbuf.at[m, core, xl, z, y], s0.at[m], r0.at[m], across)
 
     def c1(m, k, j):
         return remote(shard(m, k, 0), shard(m, k, 0), s1.at[m, k, j], r1.at[m, k, j], first_axis[k](steps[j]))
@@ -94,8 +95,9 @@
         ref = shard(m, k, -steps[j]).at[pl.ds(32 * j, 32)]
         return remote(ref, ref, s1f.at[m, k, j], r1f.at[m, k, j], first_axis[k](steps[j]))
 
-    def c2(m, k, j):
-        return remote(plane(m, k, 0), plane(m, k, 0), s2.at[m, k, j], r2.at[m, k, j], second_axis[k](steps[j]))
+    def c2(m, k, j, p):
+        ref = shard(m, k, (0, -1, 1, 2)[p])
+        return remote(ref, ref, s2.at[m, k, j, p], r2.at[m, k, j, p], second_axis[k](steps[j]))
 
     def c2f(m, k, j):
         ref = plane_half(m, k, -steps[j], j)
@@ -106,34 +108,32 @@
         return remote(ref, ref, s3.at[m, k, p], r3.at[m, k, p], sibling)
 
     def row_start(m):
-        c_local(m).wait()
         c0(m).wait_recv()
         for k, j in pairs:
             c1(m, k, j).start()
+        for k, j in pairs:
+            c2(m, k, j, 0).start()
 
     def row_pass(m):
         for k, j in pairs:
             c1(m, k, j).wait_recv()
             c1f(m, k, j).start()
+        for k, j in pairs:
+            c2(m, k, 0, 1 + j).start()
+            c2(m, k, 1, 1 + j).start()
 
     def row_end(m):
-        for k, j in pairs:
-            c1f(m, k, j).wait_recv()
-
-    def row_gather(m):
-        row_start(m)
-        row_pass(m)
-        row_end(m)
-
-    def plane_start(m):
-        for k, j in pairs:
-            c2(m, k, j).start()
         for k in range(2):
+            for j in range(2):
+                c1f(m, k, j).wait_recv()
+            c2(m, k, 0, 3).start()
+            c2(m, k, 1, 3).start()
             c3(m, k, 0).start()
 
     def plane_pass(m):
         for k, j in pairs:
-            c2(m, k, j).wait_recv()
+            for p in range(4):
+                c2(m, k, j, p).wait_recv()
             c2f(m, k, j).start()
             c3(m, k, 1 + j).start()
 
@@ -200,7 +200,18 @@
 
     for m in range(MATS):
         c_local(m).start()
-    c0(0).start()
+    greeted = [across, partner, sibling, (sp, (2 * half + 1 - xl) * 2 + 1 - core)]
+    greeted += [along_y(1), along_y(-1), along_z(1), along_z(-1)]
+    for j in range(4):
+        greeted += [((sp + 1) % 16, 4 * half + peer(j)), ((sp + 15) % 16, 4 * half + peer(j))]
+    barrier = pltpu.get_barrier_semaphore()
+    for device in greeted:
+        pl.semaphore_signal(barrier, inc=1, device_id=device, device_id_type=MESH)
+    pl.semaphore_wait(barrier, len(greeted))
+
+    for m in range(3):
+        c_local(m).wait()
+        c0(m).start()
     labels().start()
     for j in range(1, 4):
         h_halo(j).start()
@@ -217,15 +228,19 @@
         h_main_local(c).start()
         for j in range(1, 4):
             h_main(c, j).start()
-        if c == 0:
-            c0(1).start()
-    for m in range(2, MATS):
+        if c == 2:
+            c_local(3).wait()
+            c0(3).start()
+    for m in range(4, MATS):
+        c_local(m).wait()
         c0(m).start()
 
     row_start(0)
 
     zbuf[...] = jnp.zeros_like(zbuf)
     sqbuf[...] = jnp.zeros_like(sqbuf)
+    for l in range(1, LAYERS):
+        got[l * CHUNKS, 0 : LEAD * l, :] = jnp.zeros((LEAD * l, POOL), BF16)
     ext[8:24, :] = docs[...]
     labels().wait_recv()
     label_rows = []
@@ -258,10 +273,11 @@
 
     row_pass(0)
     row_end(0)
-    plane_start(0)
-    row_gather(1)
+    row_start(1)
     plane_pass(0)
-    plane_start(1)
+    row_pass(1)
+    row_start(2)
+    row_end(1)
     plane_end(0)
     weights_ready(0)
 
@@ -279,13 +295,27 @@
         at = pl.ds(pl.multiple_of(half * WIDE + b * COLS, COLS), COLS)
         return norm_gain[l : l + 1, at].astype(F32)
 
-    def send_x(s):
-        return remote(own.at[s], got.at[s], sx.at[s], rx.at[s], partner)
+    def send_x(s, skip=0):
+        rows = pl.ds(skip, CH - skip)
+        return remote(own.at[s, rows], got.at[s, rows], sx.at[s], rx.at[s], partner)
+
+    def on_x(l, c, s, act):
+        if l == 0:
+            act(send_x(s))
+        else:
+
+            @pl.when(c == 0)
+            def _():
+                act(send_x(s, LEAD * l))
+
+            @pl.when(c != 0)
+            def _():
+                act(send_x(s))
 
     def send_sq(s):
         return remote(ssown.at[s], ssgot.at[s], sq.at[s], rq.at[s], partner)
 
-    def project(l, s, squares):
+    def project(l, c, s, squares):
         sqbuf[0:CH, :] = squares
         ssown[s] = jnp.broadcast_to(jnp.sum(sqbuf[...].T, axis=0, keepdims=True), (8, 128))
         send_sq(s).start()
@@ -297,11 +327,11 @@
                 gbuf[...], rhs, (((1,), (1,)), ((), ())), preferred_element_type=F32
             )
             own[s, :, n * 256 : (n + 1) * 256] = part.astype(BF16)
-        send_x(s).start()
+        on_x(l, c, s, lambda copy: copy.start())
 
     def mix(l, c, s):
         send_sq(s).wait_recv()
-        send_x(s).wait_recv()
+        on_x(l, c, s, lambda copy: copy.wait_recv())
         scale = lax.rsqrt((ssown[s] + ssgot[s]) / D + EPS)[0:1]
         scale = jnp.broadcast_to(scale, (128, 128)).T[0:CH]
         zbuf[0:LEAD, :] = zbuf[CH : CH + LEAD, :]
@@ -317,7 +347,7 @@
             blended = jnp.dot(pooled, mix_pool[l, i], preferred_element_type=F32)
             mbuf[:, at] = (blended * pool_gain[l : l + 1, at].astype(F32)).astype(BF16)
 
-    def update(l, c, last):
+    def update(l, c):
         rows = rows_at(c)
         squares = None
         for b in range(4):
@@ -325,11 +355,23 @@
             change = jnp.dot(mbuf[...], weights, preferred_element_type=F32)
             new = (hbuf[b, rows, :].astype(F32) + change).astype(BF16)
             hbuf[b, rows, :] = new
-            if not last:
-                wide = new.astype(F32)
-                squares = squares_of(wide) if squares is None else squares + squares_of(wide)
-                gbuf[:, b * COLS : (b + 1) * COLS] = (wide * gain_of(l + 1, b)).astype(BF16)
+            wide = new.astype(F32)
+            squares = squares_of(wide) if squares is None else squares + squares_of(wide)
+            gbuf[:, b * COLS : (b + 1) * COLS] = (wide * gain_of(l + 1, b)).astype(BF16)
         return squares
+
+    def finish(c):
+        rows = rows_at(c)
+        for j in (2, 3, 1, 0):
+            b = peer(j)
+            weights = wbuf[MATS - 1, b % 2, b // 2].reshape(POOL, COLS)
+            change = jnp.dot(mbuf[...], weights, preferred_element_type=F32)
+            hbuf[b, rows, :] = (hbuf[b, rows, :].astype(F32) + change).astype(BF16)
+            for first in (True, False):
+
+                @pl.when(c == 0 if first else c != 0)
+                def _(j=j, first=first):
+                    (send_out(c, j, first) if j else keep_out(c, first)).start()
 
     def wait_rows(c):
         h_main_local(c).wait()
@@ -360,65 +402,81 @@
             wide = hbuf[b, rows, :].astype(F32)
             squares = squares_of(wide) if squares is None else squares + squares_of(wide)
             gbuf[:, b * COLS : (b + 1) * COLS] = (wide * gain_of(0, b)).astype(BF16)
-        project(0, c, squares)
+        project(0, c, c, squares)
+
+        @pl.when(c == 2)
+        def _():
+            row_pass(2)
+
         return carry
 
     lax.fori_loop(0, CHUNKS, enter, 0)
 
-    def advance(m, prepare):
-        if m + 1 < MATS and prepare:
-            row_gather(m + 1)
-        plane_pass(m)
-        if m + 1 < MATS:
-            plane_start(m + 1)
-        plane_end(m)
-        weights_ready(m)
-
-    def out_rows(c):
-        start, size = rows_of(c)
-        return start, size, mine * PART + start - HALO
-
-    def send_out(c, j):
-        start, size, base = out_rows(c)
+    plane_pass(1)
+    row_end(2)
+    row_start(3)
+    plane_end(1)
+    weights_ready(1)
+    plane_pass(2)
+    row_pass(3)
+    row_start(4)
+    plane_end(2)
+    row_end(3)
+    weights_ready(2)
+
+    def out_rows(c, quarter, first):
+        start, size = (HALO, CH - HALO) if first else (c * CH, CH)
+        base = pl.multiple_of(quarter * PART + start - HALO, 16)
+        return pl.ds(start if first else pl.multiple_of(start, 16), size), pl.ds(base, size)
+
+    def send_out(c, j, first):
+        here, there = out_rows(c, mine, first)
         to = peer(j)
         return remote(
-            hbuf.at[to, pl.ds(start, size)], out.at[pl.ds(pl.multiple_of(base, 16), size)],
-            so.at[c, j], ro.at[c, me], (sp, 4 * half + to),
+            hbuf.at[to, here], out.at[there], so.at[c, j], ro.at[c, me], (sp, 4 * half + to)
         )
 
-    def keep_out(c):
-        start, size, base = out_rows(c)
-        return pltpu.make_async_copy(
-            hbuf.at[me, pl.ds(start, size)], out.at[pl.ds(pl.multiple_of(base, 16), size)], loc_o.at[c]
-        )
-
-    def wait_out(c, j):
-        start, size, _ = out_rows(c)
+    def keep_out(c, first):
+        here, there = out_rows(c, mine, first)
+        return pltpu.make_async_copy(hbuf.at[me, here], out.at[there], loc_o.at[c])
+
+    def wait_out(c, j, first):
         frm = peer(j)
-        base = ((frm + 2 * half) % 4) * PART + start - HALO
-        ref = out.at[pl.ds(pl.multiple_of(base, 16), size)]
+        _, there = out_rows(c, (frm + 2 * half) % 4, first)
+        ref = out.at[there]
         return remote(ref, ref, so.at[c, j], ro.at[c, frm], (sp, 4 * half + frm))
 
     for l in range(LAYERS):
         last = l == LAYERS - 1
-        advance(2 * l + 1, True)
-        if not last:
-            advance(2 * l + 2, True)
+        if l == 1:
+            row_end(4)
+            plane_end(3)
+            weights_ready(3)
+            row_pass(5)
+            plane_pass(4)
+            row_end(5)
+            plane_end(4)
+            weights_ready(4)
+        if l == 2:
+            plane_end(5)
+            weights_ready(5)
 
         def one(c, carry, l=l, last=last):
             s = l * CHUNKS + c
             mix(l, c, s)
-            squares = update(l, c, last)
-            if not last:
-                project(l + 1, s + CHUNKS, squares)
+            if last:
+                finish(c)
             else:
-                for k in range(CHUNKS):
-
-                    @pl.when(c == k)
-                    def _(k=k):
-                        for j in range(1, 4):
-                            send_out(k, j).start()
-                        keep_out(k).start()
+                project(l + 1, c, s + CHUNKS, update(l, c))
+
+                @pl.when(c == (2 if l == 0 else 0))
+                def _():
+                    if l == 0:
+                        plane_pass(3)
+                        row_pass(4)
+                        row_start(5)
+                    else:
+                        plane_pass(5)
 
             return carry
 
@@ -429,7 +487,8 @@
         for k, j in pairs:
             c1(m, k, j).wait_send()
             c1f(m, k, j).wait_send()
-            c2(m, k, j).wait_send()
+            for p in range(4):
+                c2(m, k, j, p).wait_send()
             c2f(m, k, j).wait_send()
         for k in range(2):
             for p in range(4):
@@ -446,27 +505,25 @@
         for j in range(1, 4):
             h_main(c, j).wait_send()
     for s in range(LAYERS * CHUNKS):
-        send_x(s).wait_send()
+        send_x(s, LEAD * (s // CHUNKS) if s % CHUNKS == 0 else 0).wait_send()
         send_sq(s).wait_send()
     for c in range(CHUNKS):
-        keep_out(c).wait()
+        keep_out(c, c == 0).wait()
         for j in range(1, 4):
-            send_out(c, j).wait_send()
-            wait_out(c, j).wait_recv()
+            send_out(c, j, c == 0).wait_send()
+            wait_out(c, j, c == 0).wait_recv()
 
 
 def body(stream, doc_ids, norm_gain, proj_in, mix_pool, pool_gain, proj_out):
-    weights = jnp.stack([jnp.swapaxes(proj_in, 1, 2), proj_out], axis=1)
-    weights = weights.reshape(MATS, 64, COLS)
     dma = pltpu.SemaphoreType.DMA
     steps = LAYERS * CHUNKS
     vmem = pl.BlockSpec(memory_space=pltpu.VMEM)
     hbm = pl.BlockSpec(memory_space=pl.ANY)
     return pl.pallas_call(
         kernel,
-        out_shape=jax.ShapeDtypeStruct((TOK, COLS), BF16),
-        in_specs=[hbm, vmem, vmem, hbm, vmem, vmem],
-        out_specs=hbm,
+        out_shape=pltpu.VMEM((TOK, COLS), BF16),
+        in_specs=[hbm, vmem, vmem, hbm, hbm, vmem, vmem],
+        out_specs=vmem,
         scratch_shapes=[
             pltpu.VMEM((MATS, 2, 2, 4, 4, 64, COLS), BF16),
             pltpu.VMEM((4, HALO + PART, COLS), BF16),
@@ -484,17 +541,20 @@
             dma((MATS,)), dma((CHUNKS,)), dma((1,)), dma((CHUNKS,)),
             dma((MATS,)), dma((MATS,)),
             dma((MATS, 2, 2)), dma((MATS, 2, 2)), dma((MATS, 2, 2)), dma((MATS, 2, 2)),
-            dma((MATS, 2, 2)), dma((MATS, 2, 2)), dma((MATS, 2, 2)), dma((MATS, 2, 2)),
+            dma((MATS, 2, 2, 4)), dma((MATS, 2, 2, 4)), dma((MATS, 2, 2)), dma((MATS, 2, 2)),
             dma((MATS, 2, 4)), dma((MATS, 2, 4)),
             dma((CHUNKS, 4)), dma((CHUNKS, 4)), dma((4,)), dma((4,)), dma((1,)), dma((1,)),
             dma((steps,)), dma((steps,)), dma((steps,)), dma((steps,)),
             dma((CHUNKS, 4)), dma((CHUNKS, 4)),
         ],
         compiler_params=pltpu.CompilerParams(
-            has_side_effects=True, vmem_limit_bytes=56 * 1024 * 1024
+            has_side_effects=True, collective_id=0, vmem_limit_bytes=56 * 1024 * 1024
         ),
         name="mixers",
-    )(stream, doc_ids.reshape(16, 128), norm_gain, weights, mix_pool, pool_gain)
+    )(
+        stream, doc_ids.reshape(16, 128), norm_gain, jnp.swapaxes(proj_in, 1, 2), proj_out,
+        mix_pool, pool_gain,
+    )
 
 
 def solution(mesh):

time: 178 us -> 135 us (0.76)
  Pallas kernels: 173 us -> 134 us
  local copies, waits for them, and re-layouts: 3.82 us -> 1.32 us
    pallas_call x1, Pallas kernels: 173 us -> 134 us  [body(): pl.pallas_call(kernel, out_shape=pltpu.VMEM((TOK, COLS), BF16), in_specs=...]
where the time goes in v1:
time: 135 us
  Pallas kernels  134 us (99%)
    pallas_call x1, Pallas kernels, body(): pl.pallas_call(kernel, out_shape=pltpu.VMEM((TOK, COLS), BF16), in_specs=...  134 us

profile of v1, /device:TPU:1, one launch (start us, length us, event | category | flops | bytes accessed | tf_op | source)
XLA Modules:
  0.0 134.8 jit_solution(14999966896175483349)
XLA Ops:
  0.0 133.5 %mixers.1 = bf16[2048,512]{1,0:T(8,128)(2,1)S(1)} custom-call(bf16[2048,512]{1,0:T(8,128)(2,1)} %stream.1, s32[16,128]{1,0:T(8,128)} %bitcast.3, bf16[3,4096]{1,0:T(4,128)(2,1)} %norm_gain.1, bf16[3,64,512]{2,1,0:T(8,128)(2,1)} %bitcast.2, bf16[3,64,512]{2,1,0:T(8,128)(2,1)} %w_out.1, bf16[3,8,128,128]{3,2,1,0:T(8,128)(2,1)} %mix_pool.1, ...), custom_call_target="tpu_custom_call" | custom-call | tf_op jit(solution)/shard_map/mixers/pallas_call | solution.py:522
  133.5 1.3 copy.9

commit v2 on v1

--- a/solution.py
+++ b/solution.py
@@ -24,13 +24,15 @@
 CHUNKS = 5
 CH = (HALO + PART) // CHUNKS
 WINDOWS = (2, 4, 8, 16)
+STEPS = LAYERS * CHUNKS
+SPLIT = 64
 EPS = 1e-06
 
 
 def kernel(
-    stream, docs, norm_gain, w_in, w_out, mix_pool, pool_gain, out,
-    wbuf, hbuf, own, got, ssown, ssgot, gbuf, zbuf, mbuf, sqbuf, band, inv, ext,
-    loc_w, loc_h, loc_hh, loc_o,
+    stream, docs, norm_gain, w_in, w_out, mix_hbm, pool_gain, out,
+    wbuf, hbuf, own, got, ssown, ssgot, gbuf, zbuf, mbuf, sqbuf, band, inv, ext, mix_pool,
+    loc_w, loc_h, loc_hh, loc_o, loc_m,
     s0, r0, s1, r1, s1f, r1f, s2, r2, s2f, r2f, s3, r3,
     sh, rh, shh, rhh, sl, rl, sx, rx, sq, rq, so, ro,
 ):
@@ -96,7 +98,7 @@
         return remote(ref, ref, s1f.at[m, k, j], r1f.at[m, k, j], first_axis[k](steps[j]))
 
     def c2(m, k, j, p):
-        ref = shard(m, k, (0, -1, 1, 2)[p])
+        ref = shard(m, k, (0, -1, 1, 2)[p]) if m == 0 else plane(m, k, 0)
         return remote(ref, ref, s2.at[m, k, j, p], r2.at[m, k, j, p], second_axis[k](steps[j]))
 
     def c2f(m, k, j):
@@ -106,33 +108,38 @@
     def c3(m, k, p):
         ref = plane(m, k, (0, -1, 1, 2)[p])
         return remote(ref, ref, s3.at[m, k, p], r3.at[m, k, p], sibling)
+
+    def parts_of(m):
+        return range(4 if m == 0 else 1)
 
     def row_start(m):
         c0(m).wait_recv()
         for k, j in pairs:
             c1(m, k, j).start()
-        for k, j in pairs:
-            c2(m, k, j, 0).start()
+        if m == 0:
+            for k, j in pairs:
+                c2(m, k, j, 0).start()
 
     def row_pass(m):
         for k, j in pairs:
             c1(m, k, j).wait_recv()
             c1f(m, k, j).start()
-        for k, j in pairs:
-            c2(m, k, 0, 1 + j).start()
-            c2(m, k, 1, 1 + j).start()
+        if m == 0:
+            for k, j in pairs:
+                c2(m, k, 0, 1 + j).start()
+                c2(m, k, 1, 1 + j).start()
 
     def row_end(m):
         for k in range(2):
             for j in range(2):
                 c1f(m, k, j).wait_recv()
-            c2(m, k, 0, 3).start()
-            c2(m, k, 1, 3).start()
+            for j in range(2):
+                c2(m, k, j, 3 if m == 0 else 0).start()
             c3(m, k, 0).start()
 
     def plane_pass(m):
         for k, j in pairs:
-            for p in range(4):
+            for p in parts_of(m):
                 c2(m, k, j, p).wait_recv()
             c2f(m, k, j).start()
             c3(m, k, 1 + j).start()
@@ -198,26 +205,33 @@
     def labels():
         return remote(docs.at[pl.ds(15, 1)], ext.at[pl.ds(7, 1)], sl.at[0], rl.at[0], ((sp + 1) % 16, tp))
 
+    mix_copy = pltpu.make_async_copy(mix_hbm, mix_pool, loc_m.at[0])
     for m in range(MATS):
         c_local(m).start()
+    mix_copy.start()
     greeted = [across, partner, sibling, (sp, (2 * half + 1 - xl) * 2 + 1 - core)]
     greeted += [along_y(1), along_y(-1), along_z(1), along_z(-1)]
-    for j in range(4):
-        greeted += [((sp + 1) % 16, 4 * half + peer(j)), ((sp + 15) % 16, 4 * half + peer(j))]
     barrier = pltpu.get_barrier_semaphore()
     for device in greeted:
         pl.semaphore_signal(barrier, inc=1, device_id=device, device_id_type=MESH)
-    pl.semaphore_wait(barrier, len(greeted))
+
+    @pl.when(mine == 0)
+    def _():
+        for j in range(4):
+            device = ((sp + 15) % 16, 4 * half + peer(j))
+            pl.semaphore_signal(barrier, inc=1, device_id=device, device_id_type=MESH)
+
+    pl.semaphore_wait(barrier, len(greeted) + 1)
 
     for m in range(3):
         c_local(m).wait()
         c0(m).start()
-    labels().start()
     for j in range(1, 4):
         h_halo(j).start()
 
     @pl.when(mine == 0)
     def _():
+        labels().start()
         h_halo(0).start()
 
     @pl.when(mine != 0)
@@ -242,7 +256,11 @@
     for l in range(1, LAYERS):
         got[l * CHUNKS, 0 : LEAD * l, :] = jnp.zeros((LEAD * l, POOL), BF16)
     ext[8:24, :] = docs[...]
-    labels().wait_recv()
+
+    @pl.when(mine == 0)
+    def _():
+        labels().wait_recv()
+
     label_rows = []
     for k in range(5):
         row = (ext[pl.ds(4 * mine + 7 + k, 1), :] + 1).astype(F32)
@@ -274,12 +292,15 @@
     row_pass(0)
     row_end(0)
     row_start(1)
+    row_start(2)
     plane_pass(0)
     row_pass(1)
-    row_start(2)
+    row_pass(2)
+    row_start(3)
+    plane_end(0)
     row_end(1)
-    plane_end(0)
     weights_ready(0)
+    row_end(2)
 
     def rows_at(c):
         return pl.ds(pl.multiple_of(c * CH, 16), CH)
@@ -295,22 +316,37 @@
         at = pl.ds(pl.multiple_of(half * WIDE + b * COLS, COLS), COLS)
         return norm_gain[l : l + 1, at].astype(F32)
 
-    def send_x(s, skip=0):
-        rows = pl.ds(skip, CH - skip)
-        return remote(own.at[s, rows], got.at[s, rows], sx.at[s], rx.at[s], partner)
+    def send_x(s, at, rows=(0, CH), lanes=(0, POOL)):
+        index = (s, pl.ds(*rows), pl.ds(*lanes))
+        return remote(own.at[index], got.at[index], sx.at[at], rx.at[at], partner)
+
+    def x_first(n):
+        return send_x(0, STEPS + 1 + n, lanes=(n * 256, 256))
+
+    def x_kept(l, c, s):
+        if c == 0 and l > 0:
+            return [send_x(s, s, rows=(LEAD * l, CH - LEAD * l))]
+        if c == CHUNKS - 1 and l == LAYERS - 1:
+            return [send_x(s, s, rows=(0, SPLIT)), send_x(s, STEPS, rows=(SPLIT, CH - SPLIT))]
+        if c == 0:
+            return [x_first(n) for n in range(4)]
+        return [send_x(s, s)]
 
     def on_x(l, c, s, act):
-        if l == 0:
-            act(send_x(s))
-        else:
-
-            @pl.when(c == 0)
-            def _():
-                act(send_x(s, LEAD * l))
-
-            @pl.when(c != 0)
-            def _():
-                act(send_x(s))
+        special = [0, CHUNKS - 1] if l == LAYERS - 1 else [0]
+        plain = c != 0
+        for k in special:
+
+            @pl.when(c == k)
+            def _(k=k):
+                for copy in x_kept(l, k, s):
+                    act(copy)
+
+            plain = jnp.logical_and(plain, c != k)
+
+        @pl.when(plain)
+        def _():
+            act(send_x(s, s))
 
     def send_sq(s):
         return remote(ssown.at[s], ssgot.at[s], sq.at[s], rq.at[s], partner)
@@ -327,25 +363,39 @@
                 gbuf[...], rhs, (((1,), (1,)), ((), ())), preferred_element_type=F32
             )
             own[s, :, n * 256 : (n + 1) * 256] = part.astype(BF16)
-        on_x(l, c, s, lambda copy: copy.start())
-
-    def mix(l, c, s):
-        send_sq(s).wait_recv()
-        on_x(l, c, s, lambda copy: copy.wait_recv())
+            if l == 0:
+
+                @pl.when(c == 0)
+                def _(n=n):
+                    x_first(n).start()
+
+        if l == 0:
+
+            @pl.when(c != 0)
+            def _():
+                send_x(s, s).start()
+
+        else:
+            on_x(l, c, s, lambda copy: copy.start())
+
+    def mix(l, c, s, first=0, size=CH):
+        rows = slice(first, first + size)
+        here = slice(LEAD + first, LEAD + first + size)
+        if first == 0:
+            send_sq(s).wait_recv()
+            zbuf[0:LEAD, :] = zbuf[CH : CH + LEAD, :]
         scale = lax.rsqrt((ssown[s] + ssgot[s]) / D + EPS)[0:1]
-        scale = jnp.broadcast_to(scale, (128, 128)).T[0:CH]
-        zbuf[0:LEAD, :] = zbuf[CH : CH + LEAD, :]
+        scale = jnp.broadcast_to(scale, (128, 128)).T[rows]
         for i in range(GROUPS):
             at = slice(i * GROUP, (i + 1) * GROUP)
-            summed = own[s, :, at].astype(F32) + got[s, :, at].astype(F32)
-            zbuf[LEAD:, at] = (summed * scale).astype(BF16)
+            summed = own[s, rows, at].astype(F32) + got[s, rows, at].astype(F32)
+            zbuf[here, at] = (summed * scale).astype(BF16)
         for i in range(GROUPS):
             at = slice(i * GROUP, (i + 1) * GROUP)
-            values = zbuf[:, at]
-            total = jnp.dot(band[c, i % 4], values, preferred_element_type=F32)
-            pooled = (total * inv[c, i % 4] - zbuf[LEAD:, at].astype(F32)).astype(BF16)
+            total = jnp.dot(band[c, i % 4, rows], zbuf[:, at], preferred_element_type=F32)
+            pooled = (total * inv[c, i % 4, rows] - zbuf[here, at].astype(F32)).astype(BF16)
             blended = jnp.dot(pooled, mix_pool[l, i], preferred_element_type=F32)
-            mbuf[:, at] = (blended * pool_gain[l : l + 1, at].astype(F32)).astype(BF16)
+            mbuf[rows, at] = (blended * pool_gain[l : l + 1, at].astype(F32)).astype(BF16)
 
     def update(l, c):
         rows = rows_at(c)
@@ -360,18 +410,22 @@
             gbuf[:, b * COLS : (b + 1) * COLS] = (wide * gain_of(l + 1, b)).astype(BF16)
         return squares
 
-    def finish(c):
-        rows = rows_at(c)
+    def finish(c, first=0, size=CH):
         for j in (2, 3, 1, 0):
             b = peer(j)
             weights = wbuf[MATS - 1, b % 2, b // 2].reshape(POOL, COLS)
-            change = jnp.dot(mbuf[...], weights, preferred_element_type=F32)
+            change = jnp.dot(mbuf[first : first + size], weights, preferred_element_type=F32)
+            rows = pl.ds(pl.multiple_of(c * CH + first, 16), size)
             hbuf[b, rows, :] = (hbuf[b, rows, :].astype(F32) + change).astype(BF16)
-            for first in (True, False):
-
-                @pl.when(c == 0 if first else c != 0)
-                def _(j=j, first=first):
-                    (send_out(c, j, first) if j else keep_out(c, first)).start()
+            if isinstance(c, int):
+                at = c + (first > 0)
+                (send_out(at, j, c * CH + first, size) if j else keep_out(at, c * CH + first, size)).start()
+                continue
+            for start, size_ in ((HALO, CH - HALO), (pl.multiple_of(c * CH, 16), CH)):
+
+                @pl.when(c == 0 if size_ < CH else c != 0)
+                def _(j=j, start=start, size_=size_):
+                    (send_out(c, j, start, size_) if j else keep_out(c, start, size_)).start()
 
     def wait_rows(c):
         h_main_local(c).wait()
@@ -406,53 +460,50 @@
 
         @pl.when(c == 2)
         def _():
-            row_pass(2)
+            row_pass(3)
 
         return carry
 
     lax.fori_loop(0, CHUNKS, enter, 0)
 
     plane_pass(1)
-    row_end(2)
-    row_start(3)
+    row_start(4)
+    plane_pass(2)
+    row_end(3)
     plane_end(1)
     weights_ready(1)
-    plane_pass(2)
-    row_pass(3)
-    row_start(4)
+    row_pass(4)
+    row_start(5)
     plane_end(2)
-    row_end(3)
     weights_ready(2)
 
-    def out_rows(c, quarter, first):
-        start, size = (HALO, CH - HALO) if first else (c * CH, CH)
+    def out_rows(quarter, start, size):
         base = pl.multiple_of(quarter * PART + start - HALO, 16)
-        return pl.ds(start if first else pl.multiple_of(start, 16), size), pl.ds(base, size)
-
-    def send_out(c, j, first):
-        here, there = out_rows(c, mine, first)
+        return pl.ds(start, size), pl.ds(base, size)
+
+    def send_out(at, j, start, size):
+        here, there = out_rows(mine, start, size)
         to = peer(j)
         return remote(
-            hbuf.at[to, here], out.at[there], so.at[c, j], ro.at[c, me], (sp, 4 * half + to)
+            hbuf.at[to, here], out.at[there], so.at[at, j], ro.at[at, me], (sp, 4 * half + to)
         )
 
-    def keep_out(c, first):
-        here, there = out_rows(c, mine, first)
-        return pltpu.make_async_copy(hbuf.at[me, here], out.at[there], loc_o.at[c])
-
-    def wait_out(c, j, first):
+    def keep_out(at, start, size):
+        here, there = out_rows(mine, start, size)
+        return pltpu.make_async_copy(hbuf.at[me, here], out.at[there], loc_o.at[at])
+
+    def wait_out(at, j, start, size):
         frm = peer(j)
-        _, there = out_rows(c, (frm + 2 * half) % 4, first)
+        _, there = out_rows((frm + 2 * half) % 4, start, size)
         ref = out.at[there]
-        return remote(ref, ref, so.at[c, j], ro.at[c, frm], (sp, 4 * half + frm))
-
+        return remote(ref, ref, so.at[at, j], ro.at[at, frm], (sp, 4 * half + frm))
+
+    mix_copy.wait()
     for l in range(LAYERS):
         last = l == LAYERS - 1
         if l == 1:
-            row_end(4)
             plane_end(3)
             weights_ready(3)
-            row_pass(5)
             plane_pass(4)
             row_end(5)
             plane_end(4)
@@ -463,66 +514,80 @@
 
         def one(c, carry, l=l, last=last):
             s = l * CHUNKS + c
+            on_x(l, c, s, lambda copy: copy.wait_recv())
             mix(l, c, s)
             if last:
                 finish(c)
             else:
                 project(l + 1, c, s + CHUNKS, update(l, c))
 
-                @pl.when(c == (2 if l == 0 else 0))
+                @pl.when(c == 1)
                 def _():
-                    if l == 0:
-                        plane_pass(3)
-                        row_pass(4)
-                        row_start(5)
-                    else:
-                        plane_pass(5)
+                    plane_pass(3 if l == 0 else 5)
+
+                if l == 0:
+
+                    @pl.when(c == 2)
+                    def _():
+                        row_end(4)
+                        row_pass(5)
 
             return carry
 
-        lax.fori_loop(0, CHUNKS, one, 0)
+        lax.fori_loop(0, CHUNKS - 1 if last else CHUNKS, one, 0)
+
+    end = CHUNKS - 1
+    for n, (first, size) in enumerate(((0, SPLIT), (SPLIT, CH - SPLIT))):
+        x_kept(LAYERS - 1, end, STEPS - 1)[n].wait_recv()
+        mix(LAYERS - 1, end, STEPS - 1, first, size)
+        finish(end, first, size)
 
     for m in range(MATS):
         c0(m).wait_send()
         for k, j in pairs:
             c1(m, k, j).wait_send()
             c1f(m, k, j).wait_send()
-            for p in range(4):
+            for p in parts_of(m):
                 c2(m, k, j, p).wait_send()
             c2f(m, k, j).wait_send()
         for k in range(2):
             for p in range(4):
                 c3(m, k, p).wait_send()
-    labels().wait_send()
     for j in range(1, 4):
         h_halo(j).wait_send()
 
     @pl.when(mine == 0)
     def _():
+        labels().wait_send()
         h_halo(0).wait_send()
 
     for c in range(CHUNKS):
         for j in range(1, 4):
             h_main(c, j).wait_send()
-    for s in range(LAYERS * CHUNKS):
-        send_x(s, LEAD * (s // CHUNKS) if s % CHUNKS == 0 else 0).wait_send()
-        send_sq(s).wait_send()
-    for c in range(CHUNKS):
-        keep_out(c, c == 0).wait()
+    for l in range(LAYERS):
+        for c in range(CHUNKS):
+            s = l * CHUNKS + c
+            for copy in x_kept(l, c, s):
+                copy.wait_send()
+            send_sq(s).wait_send()
+    pieces = [(HALO, CH - HALO)] + [(c * CH, CH) for c in range(1, CHUNKS - 1)]
+    pieces += [(end * CH, SPLIT), (end * CH + SPLIT, CH - SPLIT)]
+    for at, (start, size) in enumerate(pieces):
+        keep_out(at, start, size).wait()
         for j in range(1, 4):
-            send_out(c, j, c == 0).wait_send()
-            wait_out(c, j, c == 0).wait_recv()
+            send_out(at, j, start, size).wait_send()
+            wait_out(at, j, start, size).wait_recv()
 
 
 def body(stream, doc_ids, norm_gain, proj_in, mix_pool, pool_gain, proj_out):
     dma = pltpu.SemaphoreType.DMA
-    steps = LAYERS * CHUNKS
+    steps = STEPS
     vmem = pl.BlockSpec(memory_space=pltpu.VMEM)
     hbm = pl.BlockSpec(memory_space=pl.ANY)
     return pl.pallas_call(
         kernel,
         out_shape=pltpu.VMEM((TOK, COLS), BF16),
-        in_specs=[hbm, vmem, vmem, hbm, hbm, vmem, vmem],
+        in_specs=[hbm, vmem, vmem, hbm, hbm, hbm, vmem],
         out_specs=vmem,
         scratch_shapes=[
             pltpu.VMEM((MATS, 2, 2, 4, 4, 64, COLS), BF16),
@@ -538,14 +603,15 @@
             pltpu.VMEM((CHUNKS, 4, CH, 128), BF16),
             pltpu.VMEM((CHUNKS, 4, CH, 128), F32),
             pltpu.VMEM((24, 128), jnp.int32),
-            dma((MATS,)), dma((CHUNKS,)), dma((1,)), dma((CHUNKS,)),
+            pltpu.VMEM((LAYERS, GROUPS, GROUP, GROUP), BF16),
+            dma((MATS,)), dma((CHUNKS,)), dma((1,)), dma((CHUNKS + 1,)), dma((1,)),
             dma((MATS,)), dma((MATS,)),
             dma((MATS, 2, 2)), dma((MATS, 2, 2)), dma((MATS, 2, 2)), dma((MATS, 2, 2)),
             dma((MATS, 2, 2, 4)), dma((MATS, 2, 2, 4)), dma((MATS, 2, 2)), dma((MATS, 2, 2)),
             dma((MATS, 2, 4)), dma((MATS, 2, 4)),
             dma((CHUNKS, 4)), dma((CHUNKS, 4)), dma((4,)), dma((4,)), dma((1,)), dma((1,)),
-            dma((steps,)), dma((steps,)), dma((steps,)), dma((steps,)),
-            dma((CHUNKS, 4)), dma((CHUNKS, 4)),
+            dma((steps + 5,)), dma((steps + 5,)), dma((steps,)), dma((steps,)),
+            dma((CHUNKS + 1, 4)), dma((CHUNKS + 1, 4)),
         ],
         compiler_params=pltpu.CompilerParams(
             has_side_effects=True, collective_id=0, vmem_limit_bytes=56 * 1024 * 1024

time: 135 us -> 130 us (0.963)
  Pallas kernels: 134 us -> 128 us
    pallas_call x1, Pallas kernels: 134 us -> 128 us  [body(): pl.pallas_call(kernel, out_shape=pltpu.VMEM((TOK, COLS), BF16), in_specs=...]
where the time goes in v2:
time: 130 us
  Pallas kernels  128 us (98%)
  local copies, waits for them, and re-layouts  1.32 us (1%)
    pallas_call x1, Pallas kernels, body(): pl.pallas_call(kernel, out_shape=pltpu.VMEM((TOK, COLS), BF16), in_specs=...  128 us

profile of v2, /device:TPU:1, one launch (start us, length us, event | category | flops | bytes accessed | tf_op | source)
XLA Modules:
  0.0 129.8 jit_solution(12974228425520758503)
XLA Ops:
  0.0 128.5 %mixers.1 = bf16[2048,512]{1,0:T(8,128)(2,1)S(1)} custom-call(bf16[2048,512]{1,0:T(8,128)(2,1)} %stream.1, s32[16,128]{1,0:T(8,128)} %bitcast.3, bf16[3,4096]{1,0:T(4,128)(2,1)} %norm_gain.1, bf16[3,64,512]{2,1,0:T(8,128)(2,1)} %bitcast.2, bf16[3,64,512]{2,1,0:T(8,128)(2,1)} %w_out.1, bf16[3,8,128,128]{3,2,1,0:T(8,128)(2,1)} %mix_hbm.1, ...), custom_call_target="tpu_custom_call" | custom-call | tf_op jit(solution)/shard_map/mixers/pallas_call | solution.py:587
  128.5 1.3 %copy.9 = bf16[2048,512]{1,0:T(8,128)(2,1)} copy(bf16[2048,512]{1,0:T(8,128)(2,1)S(1)} %mixers.1) | data formatting | bytes 4194304

commit v3 on v2

--- a/solution.py
+++ b/solution.py
@@ -351,32 +351,28 @@
     def send_sq(s):
         return remote(ssown.at[s], ssgot.at[s], sq.at[s], rq.at[s], partner)
 
-    def project(l, c, s, squares):
+    def share_squares(s, squares):
         sqbuf[0:CH, :] = squares
         ssown[s] = jnp.broadcast_to(jnp.sum(sqbuf[...].T, axis=0, keepdims=True), (8, 128))
         send_sq(s).start()
+
+    def project(l, chunks):
+        rows = slice(chunks[0] * CH, (chunks[-1] + 1) * CH)
         for n in range(4):
             rhs = jnp.concatenate(
                 [wbuf[2 * l, b % 2, b // 2, n].reshape(256, COLS) for b in range(4)], axis=1
             )
             part = lax.dot_general(
-                gbuf[...], rhs, (((1,), (1,)), ((), ())), preferred_element_type=F32
-            )
-            own[s, :, n * 256 : (n + 1) * 256] = part.astype(BF16)
-            if l == 0:
-
-                @pl.when(c == 0)
-                def _(n=n):
+                gbuf[rows, :], rhs, (((1,), (1,)), ((), ())), preferred_element_type=F32
+            ).astype(BF16)
+            for k, c in enumerate(chunks):
+                own[l * CHUNKS + c, :, n * 256 : (n + 1) * 256] = part[k * CH : (k + 1) * CH]
+                if l == 0 and c == 0:
                     x_first(n).start()
-
-        if l == 0:
-
-            @pl.when(c != 0)
-            def _():
-                send_x(s, s).start()
-
-        else:
-            on_x(l, c, s, lambda copy: copy.start())
+        for c in chunks:
+            if l > 0 or c > 0:
+                for copy in x_kept(l, c, l * CHUNKS + c):
+                    copy.start()
 
     def mix(l, c, s, first=0, size=CH):
         rows = slice(first, first + size)
@@ -407,7 +403,7 @@
             hbuf[b, rows, :] = new
             wide = new.astype(F32)
             squares = squares_of(wide) if squares is None else squares + squares_of(wide)
-            gbuf[:, b * COLS : (b + 1) * COLS] = (wide * gain_of(l + 1, b)).astype(BF16)
+            gbuf[rows, b * COLS : (b + 1) * COLS] = (wide * gain_of(l + 1, b)).astype(BF16)
         return squares
 
     def finish(c, first=0, size=CH):
@@ -455,18 +451,26 @@
         for b in range(4):
             wide = hbuf[b, rows, :].astype(F32)
             squares = squares_of(wide) if squares is None else squares + squares_of(wide)
-            gbuf[:, b * COLS : (b + 1) * COLS] = (wide * gain_of(0, b)).astype(BF16)
-        project(0, c, c, squares)
+            gbuf[rows, b * COLS : (b + 1) * COLS] = (wide * gain_of(0, b)).astype(BF16)
+        share_squares(c, squares)
 
         @pl.when(c == 2)
         def _():
+            project(0, (0, 1, 2))
             row_pass(3)
 
+        @pl.when(c == 3)
+        def _():
+            plane_pass(1)
+
+        @pl.when(c == 4)
+        def _():
+            project(0, (3, 4))
+
         return carry
 
     lax.fori_loop(0, CHUNKS, enter, 0)
 
-    plane_pass(1)
     row_start(4)
     plane_pass(2)
     row_end(3)
@@ -519,10 +523,11 @@
             if last:
                 finish(c)
             else:
-                project(l + 1, c, s + CHUNKS, update(l, c))
+                share_squares(s + CHUNKS, update(l, c))
 
                 @pl.when(c == 1)
                 def _():
+                    project(l + 1, (0, 1))
                     plane_pass(3 if l == 0 else 5)
 
                 if l == 0:
@@ -531,6 +536,10 @@
                     def _():
                         row_end(4)
                         row_pass(5)
+
+                @pl.when(c == 4)
+                def _():
+                    project(l + 1, (2, 3, 4))
 
             return carry
 
@@ -596,7 +605,7 @@
             pltpu.VMEM((steps, CH, POOL), BF16),
             pltpu.VMEM((steps, 8, 128), F32),
             pltpu.VMEM((steps, 8, 128), F32),
-            pltpu.VMEM((CH, WIDE), BF16),
+            pltpu.VMEM((CHUNKS * CH, WIDE), BF16),
             pltpu.VMEM((LEAD + CH, POOL), BF16),
             pltpu.VMEM((CH, POOL), BF16),
             pltpu.VMEM((128, 128), F32),

time: 130 us -> 122 us (0.938)
  Pallas kernels: 128 us -> 121 us
    pallas_call x1, Pallas kernels: 128 us -> 121 us  [body(): pl.pallas_call(kernel, out_shape=pltpu.VMEM((TOK, COLS), BF16), in_specs=...]
where the time goes in v3:
time: 122 us
  Pallas kernels  121 us (99%)
  local copies, waits for them, and re-layouts  1.32 us (1%)
    pallas_call x1, Pallas kernels, body(): pl.pallas_call(kernel, out_shape=pltpu.VMEM((TOK, COLS), BF16), in_specs=...  121 us

profile of v3, /device:TPU:1, one launch (start us, length us, event | category | flops | bytes accessed | tf_op | source)
XLA Modules:
  0.0 122.3 jit_solution(2401480611490340473)
XLA Ops:
  0.0 120.9 %mixers.1 = bf16[2048,512]{1,0:T(8,128)(2,1)S(1)} custom-call(bf16[2048,512]{1,0:T(8,128)(2,1)} %stream.1, s32[16,128]{1,0:T(8,128)} %bitcast.3, bf16[3,4096]{1,0:T(4,128)(2,1)} %norm_gain.1, bf16[3,64,512]{2,1,0:T(8,128)(2,1)} %bitcast.2, bf16[3,64,512]{2,1,0:T(8,128)(2,1)} %w_out.1, bf16[3,8,128,128]{3,2,1,0:T(8,128)(2,1)} %mix_hbm.1, ...), custom_call_target="tpu_custom_call" | custom-call | tf_op jit(solution)/shard_map/mixers/pallas_call | solution.py:596
  121.0 1.3 %copy.9 = bf16[2048,512]{1,0:T(8,128)(2,1)} copy(bf16[2048,512]{1,0:T(8,128)(2,1)S(1)} %mixers.1) | data formatting | bytes 4194304

commit v4 on v3

--- a/solution.py
+++ b/solution.py
@@ -454,9 +454,13 @@
             gbuf[rows, b * COLS : (b + 1) * COLS] = (wide * gain_of(0, b)).astype(BF16)
         share_squares(c, squares)
 
+        @pl.when(c == 1)
+        def _():
+            project(0, (0, 1))
+
         @pl.when(c == 2)
         def _():
-            project(0, (0, 1, 2))
+            project(0, (2,))
             row_pass(3)
 
         @pl.when(c == 3)
@@ -478,8 +482,6 @@
     weights_ready(1)
     row_pass(4)
     row_start(5)
-    plane_end(2)
-    weights_ready(2)
 
     def out_rows(quarter, start, size):
         base = pl.multiple_of(quarter * PART + start - HALO, 16)
@@ -506,12 +508,9 @@
     for l in range(LAYERS):
         last = l == LAYERS - 1
         if l == 1:
+            row_end(5)
             plane_end(3)
             weights_ready(3)
-            plane_pass(4)
-            row_end(5)
-            plane_end(4)
-            weights_ready(4)
         if l == 2:
             plane_end(5)
             weights_ready(5)
@@ -525,21 +524,38 @@
             else:
                 share_squares(s + CHUNKS, update(l, c))
 
-                @pl.when(c == 1)
+                if l == 0:
+
+                    @pl.when(c == 1)
+                    def _():
+                        plane_end(2)
+
+                    @pl.when(c == 3)
+                    def _():
+                        plane_pass(3)
+                        row_pass(5)
+                        row_end(4)
+
+                else:
+
+                    @pl.when(c == 0)
+                    def _():
+                        plane_pass(4)
+
+                    @pl.when(c == 1)
+                    def _():
+                        plane_pass(5)
+
+                @pl.when(c == 2)
                 def _():
-                    project(l + 1, (0, 1))
-                    plane_pass(3 if l == 0 else 5)
-
-                if l == 0:
-
-                    @pl.when(c == 2)
-                    def _():
-                        row_end(4)
-                        row_pass(5)
+                    if l == 1:
+                        plane_end(4)
+                    weights_ready(2 * l + 2)
+                    project(l + 1, (0, 1, 2))
 
                 @pl.when(c == 4)
                 def _():
-                    project(l + 1, (2, 3, 4))
+                    project(l + 1, (3, 4))
 
             return carry
 

time: 122 us -> 121 us (level)
  no operation moved by 1% of the time
where the time goes in v4:
time: 121 us
  Pallas kernels  120 us (99%)
  local copies, waits for them, and re-layouts  1.32 us (1%)
    pallas_call x1, Pallas kernels, body(): pl.pallas_call(kernel, out_shape=pltpu.VMEM((TOK, COLS), BF16), in_specs=...  120 us

profile of v4, /device:TPU:1, one launch (start us, length us, event | category | flops | bytes accessed | tf_op | source)
XLA Modules:
  0.0 121.1 jit_solution(2563714380664397823)
XLA Ops:
  0.0 119.8 %mixers.1 = bf16[2048,512]{1,0:T(8,128)(2,1)S(1)} custom-call(bf16[2048,512]{1,0:T(8,128)(2,1)} %stream.1, s32[16,128]{1,0:T(8,128)} %bitcast.3, bf16[3,4096]{1,0:T(4,128)(2,1)} %norm_gain.1, bf16[3,64,512]{2,1,0:T(8,128)(2,1)} %bitcast.2, bf16[3,64,512]{2,1,0:T(8,128)(2,1)} %w_out.1, bf16[3,8,128,128]{3,2,1,0:T(8,128)(2,1)} %mix_hbm.1, ...), custom_call_target="tpu_custom_call" | custom-call | tf_op jit(solution)/shard_map/mixers/pallas_call | solution.py:612
  119.8 1.3 %copy.9 = bf16[2048,512]{1,0:T(8,128)(2,1)} copy(bf16[2048,512]{1,0:T(8,128)(2,1)S(1)} %mixers.1) | data formatting | bytes 4194304

commit v5 on v4

--- a/solution.py
+++ b/solution.py
@@ -243,9 +243,10 @@
         for j in range(1, 4):
             h_main(c, j).start()
         if c == 2:
-            c_local(3).wait()
-            c0(3).start()
-    for m in range(4, MATS):
+            for m in (3, 4):
+                c_local(m).wait()
+                c0(m).start()
+    for m in range(5, MATS):
         c_local(m).wait()
         c0(m).start()
 

time: 121 us -> 121 us (level)
  no operation moved by 1% of the time
where the time goes in v5:
time: 121 us
  Pallas kernels  119 us (98%)
  local copies, waits for them, and re-layouts  1.32 us (1%)
    pallas_call x1, Pallas kernels, body(): pl.pallas_call(kernel, out_shape=pltpu.VMEM((TOK, COLS), BF16), in_specs=...  119 us

profile of v5, /device:TPU:1, one launch (start us, length us, event | category | flops | bytes accessed | tf_op | source)
XLA Modules:
  0.0 120.8 jit_solution(15552611567688608483)
XLA Ops:
  0.0 119.5 %mixers.1 = bf16[2048,512]{1,0:T(8,128)(2,1)S(1)} custom-call(bf16[2048,512]{1,0:T(8,128)(2,1)} %stream.1, s32[16,128]{1,0:T(8,128)} %bitcast.3, bf16[3,4096]{1,0:T(4,128)(2,1)} %norm_gain.1, bf16[3,64,512]{2,1,0:T(8,128)(2,1)} %bitcast.2, bf16[3,64,512]{2,1,0:T(8,128)(2,1)} %w_out.1, bf16[3,8,128,128]{3,2,1,0:T(8,128)(2,1)} %mix_hbm.1, ...), custom_call_target="tpu_custom_call" | custom-call | tf_op jit(solution)/shard_map/mixers/pallas_call | solution.py:613
  119.5 1.3 %copy.9 = bf16[2048,512]{1,0:T(8,128)(2,1)} copy(bf16[2048,512]{1,0:T(8,128)(2,1)S(1)} %mixers.1) | data formatting | bytes 4194304
